TPU v7x, 512 devices: a whole 4x4x16 slice. The times are simulated.
512 devices in a mesh: fs: 32 (over z, core), tp: 16 (over y, x).
Axes of the slice: x: 4, y: 4, z: 16, core: 2. Of those that a mesh axis runs over, the one named last changes fastest.
Arguments:
- late_input: bfloat16 [4096, 2048], P('fs'), may hold values from -6 to 6
- early_input: bfloat16 [4096, 2048], P('fs'), may hold values from -6 to 6
- early_mid: bfloat16 [4096, 2048], P('fs'), may hold values from -6 to 6
- cotangent: bfloat16 [4096, 2048], P('fs'), may hold values from -6 to 6
- gain_first: float32 [2048], replicated, may hold values from 0.1 to 1.9
- gain_second: float32 [2048], replicated, may hold values from 0.1 to 1.9
- gate_first: bfloat16 [2048, 2816], P('fs', 'tp'), may hold values from -0.125 to 0.125
- up_first: bfloat16 [2048, 2816], P('fs', 'tp'), may hold values from -0.125 to 0.125
- down_first: bfloat16 [2816, 2048], P('tp', 'fs'), may hold values from -0.109375 to 0.109375
- gate_second: bfloat16 [2048, 2816], P('fs', 'tp'), may hold values from -0.125 to 0.125
- up_second: bfloat16 [2048, 2816], P('fs', 'tp'), may hold values from -0.125 to 0.125
- down_second: bfloat16 [2816, 2048], P('tp', 'fs'), may hold values from -0.109375 to 0.109375
- sum_gate_first: float32 [2048, 2816], P('fs', 'tp'), may hold values from -256 to 256
- sum_up_first: float32 [2048, 2816], P('fs', 'tp'), may hold values from -256 to 256
- sum_down_first: float32 [2816, 2048], P('tp', 'fs'), may hold values from -256 to 256
- sum_gate_second: float32 [2048, 2816], P('fs', 'tp'), may hold values from -256 to 256
- sum_up_second: float32 [2048, 2816], P('fs', 'tp'), may hold values from -256 to 256
- sum_down_second: float32 [2816, 2048], P('tp', 'fs'), may hold values from -256 to 256
Outputs:
- late_mid: bfloat16 [4096, 2048], P('fs')
- late_out: bfloat16 [4096, 2048], P('fs')
- input_grad: bfloat16 [4096, 2048], P('fs')
- new_gate_first: float32 [2048, 2816], P('fs', 'tp')
- new_up_first: float32 [2048, 2816], P('fs', 'tp')
- new_down_first: float32 [2816, 2048], P('tp', 'fs')
- new_gate_second: float32 [2048, 2816], P('fs', 'tp')
- new_up_second: float32 [2048, 2816], P('fs', 'tp')
- new_down_second: float32 [2816, 2048], P('tp', 'fs')
All inputs are finite; a program needn't handle non-finite values.
Results may differ from a plain program's by a relative error of at most 0.015.
Values may be sent and summed in bfloat16 or wider, within the bound.
No kernel may reach another device: no remote copies, remote signals or barrier semaphores. Data moves between devices by JAX's collectives and lax.ppermute only.
A program may use at most 128 MiB of HBM per device.

v0:
```python
import jax
import jax.numpy as jnp
from jax import lax
from jax.sharding import PartitionSpec as P

norm_eps = 1e-06


def sent_together(arrays, axis, dim, along):
    both = jnp.concatenate(arrays, axis=along)
    whole, at, outs = (lax.all_gather(both, axis, axis=dim, tiled=True), 0, [])
    for a in arrays:
        outs.append(lax.slice_in_dim(whole, at, at + a.shape[along], axis=along))
        at += a.shape[along]
    return tuple(outs)


def gather_turned(arrays, axis, dims):
    turned = [jnp.moveaxis(a, dim, 0) for a, dim in zip(arrays, dims)]
    widths = [t[0].size for t in turned]
    both = jnp.concatenate([t.reshape(-1, w) for t, w in zip(turned, widths)], axis=1)
    whole = lax.all_gather(both, axis, axis=0, tiled=True)
    blocks = jnp.split(whole, [sum(widths[:k]) for k in range(1, len(widths))], axis=1)
    return tuple(
        (
            jnp.moveaxis(b.reshape(-1, *t.shape[1:]), 0, dim)
            for b, t, dim in zip(blocks, turned, dims)
        )
    )


def normalize(values, gain_vector):
    widened = values.astype(jnp.float32)
    factor = lax.rsqrt(jnp.mean(widened * widened, axis=-1, keepdims=True) + norm_eps)
    normed = (widened * factor * gain_vector).astype(jnp.bfloat16)
    return (widened, factor, normed)


def block_forward(values, params):
    gain_vector, w_gate, w_up, w_down = params
    widened, factor, normed = normalize(values, gain_vector)
    gate_pre = jnp.dot(normed, w_gate, preferred_element_type=jnp.float32)
    up_pre = jnp.dot(normed, w_up, preferred_element_type=jnp.float32)
    hidden = (jax.nn.silu(gate_pre) * up_pre).astype(jnp.bfloat16)
    branch = lax.psum(
        jnp.dot(hidden, w_down, preferred_element_type=jnp.float32).astype(jnp.bfloat16), "tp"
    ).astype(jnp.float32)
    return (widened + 0.5 * branch).astype(jnp.bfloat16)


def block_backward(values, cotangent, params):
    gain_vector, w_gate, w_up, w_down = params
    widened, factor, normed = normalize(values, gain_vector)
    gate_pre = jnp.dot(normed, w_gate, preferred_element_type=jnp.float32)
    up_pre = jnp.dot(normed, w_up, preferred_element_type=jnp.float32)
    sigmoid_gate = jax.nn.sigmoid(gate_pre)
    activated = gate_pre * sigmoid_gate
    hidden = (activated * up_pre).astype(jnp.bfloat16)
    hidden_grad = 0.5 * jnp.einsum(
        "td,fd->tf", cotangent, w_down, preferred_element_type=jnp.float32
    )
    gate_grad = (
        hidden_grad * up_pre * sigmoid_gate * (1.0 + gate_pre * (1.0 - sigmoid_gate))
    ).astype(jnp.bfloat16)
    up_grad = (hidden_grad * activated).astype(jnp.bfloat16)
    partial_value = jnp.einsum("tf,df->td", gate_grad, w_gate, preferred_element_type=jnp.float32)
    partial_value = partial_value + jnp.einsum(
        "tf,df->td", up_grad, w_up, preferred_element_type=jnp.float32
    )
    normed_grad = lax.psum(partial_value.astype(jnp.bfloat16), "tp").astype(jnp.float32)
    scaled = normed_grad * gain_vector
    unit_rows = widened * factor
    rows_grad = cotangent.astype(jnp.float32) + factor * (
        scaled - unit_rows * jnp.mean(scaled * unit_rows, axis=-1, keepdims=True)
    )
    return (rows_grad, (normed, cotangent, gate_grad, up_grad, hidden))


def fold_pair(pieces, columns_in):
    return (
        jnp.einsum("td,tf->df", columns_in, pieces[0], preferred_element_type=jnp.float32),
        jnp.einsum("td,tf->df", columns_in, pieces[1], preferred_element_type=jnp.float32),
    )


def fold_block(pieces, columns_in, columns_out):
    paired = fold_pair(pieces[0:2], columns_in)
    return paired + (
        jnp.einsum("tf,td->fd", pieces[2], columns_out, preferred_element_type=jnp.float32),
    )


def per_device(
    late_input,
    early_input,
    early_mid,
    cotangent,
    gain_first,
    gain_second,
    gate_first,
    up_first,
    down_first,
    gate_second,
    up_second,
    down_second,
    sum_gate_first,
    sum_up_first,
    sum_down_first,
    sum_gate_second,
    sum_up_second,
    sum_down_second,
):
    rows_in = sent_together((gate_first, up_first, gate_second, up_second), "fs", 0, 1)
    cols_out = gather_turned((down_first, down_second), "fs", (1, 1))
    first_params = (gain_first, rows_in[0], rows_in[1], cols_out[0])
    second_params = (gain_second, rows_in[2], rows_in[3], cols_out[1])
    late_mid = block_forward(late_input, first_params)
    late_out = block_forward(late_mid, second_params)
    mid_grad, saved_second = block_backward(early_mid, cotangent, second_params)
    mid_grad = mid_grad.astype(jnp.bfloat16)
    rows_grad, saved_first = block_backward(early_input, mid_grad, first_params)
    pieces = sent_together(
        (
            saved_second[2],
            saved_second[3],
            saved_second[4],
            saved_first[2],
            saved_first[3],
            saved_first[4],
        ),
        "fs",
        0,
        1,
    )
    upper = fold_block(
        pieces[0:3],
        lax.all_to_all(saved_second[0], "fs", split_axis=1, concat_axis=0, tiled=True),
        lax.all_to_all(saved_second[1], "fs", split_axis=1, concat_axis=0, tiled=True),
    )
    lower = fold_block(
        pieces[3:6],
        lax.all_to_all(saved_first[0], "fs", split_axis=1, concat_axis=0, tiled=True),
        lax.all_to_all(saved_first[1], "fs", split_axis=1, concat_axis=0, tiled=True),
    )
    result = upper + lower
    grads_second = (result[0], result[1], 0.5 * result[2])
    grads_first = (result[3], result[4], 0.5 * result[5])
    return (
        late_mid,
        late_out,
        rows_grad.astype(jnp.bfloat16),
        sum_gate_first + grads_first[0],
        sum_up_first + grads_first[1],
        sum_down_first + grads_first[2],
        sum_gate_second + grads_second[0],
        sum_up_second + grads_second[1],
        sum_down_second + grads_second[2],
    )


def solution(mesh):
    in_specs = (
        P("fs", None),
        P("fs", None),
        P("fs", None),
        P("fs", None),
        P(),
        P(),
        P("fs", "tp"),
        P("fs", "tp"),
        P("tp", "fs"),
        P("fs", "tp"),
        P("fs", "tp"),
        P("tp", "fs"),
        P("fs", "tp"),
        P("fs", "tp"),
        P("tp", "fs"),
        P("fs", "tp"),
        P("fs", "tp"),
        P("tp", "fs"),
    )
    out_specs = (
        P("fs", None),
        P("fs", None),
        P("fs", None),
        P("fs", "tp"),
        P("fs", "tp"),
        P("tp", "fs"),
        P("fs", "tp"),
        P("fs", "tp"),
        P("tp", "fs"),
    )
    return jax.shard_map(
        per_device, mesh=mesh, in_specs=in_specs, out_specs=out_specs, check_vma=False
    )
```

profile of v0, /device:TPU:1, one launch (start us, length us, event | category | flops | bytes accessed | tf_op | source)
XLA Modules:
  0.0 560.9 jit_solution(5887314163387625684)
XLA Ops:
  8.8 1.6 pad_maximum_fusion
  14.1 2.0 fusion.47
  16.1 71.3 %all-gather.6.cloned.1.call-done = bf16[2048,352]{1,0:T(8,128)(2,1)} async-done(((bf16[64,352]{1,0:T(8,128)(2,1)}), bf16[2048,352]{1,0:T(8,128)(2,1)}) %all-gather.6.cloned.1.call-update) | async-done | bytes 1441808 | tf_op jit(solution)/shard_map/all_gather | solution.py:22
  87.5 2.1 fusion.20
  89.6 70.4 %all-gather.4.cloned.1.call-done = bf16[2048,704]{1,0:T(8,128)(2,1)} async-done(((bf16[64,704]{1,0:T(8,128)(2,1)}), bf16[2048,704]{1,0:T(8,128)(2,1)}) %all-gather.4.cloned.1.call-update) | async-done | bytes 2883600 | tf_op jit(solution)/shard_map/all_gather | solution.py:11
  160.0 2.6 fusion.74
  162.6 3.2 constant_dynamic-update-slice_fusion.3
  166.5 1.6 fusion.93
  168.1 3.9 convolution_convert_fusion.1
  177.5 110.1 %all-reduce.7.cloned.1.call-done = (bf16[128,2048]{1,0:T(8,128)(2,1)}, bf16[128,2048]{1,0:T(8,128)(2,1)}) async-done(((bf16[128,2048]{1,0:T(8,128)(2,1)}, bf16[128,2048]{1,0:T(8,128)(2,1)}), (bf16[128,2048]{1,0:T(8,128)(2,1)}, bf16[128,2048]{1,0:T(8,128)(2,1)})) %all-reduce.7.cloned.1.call-update) | async-done | bytes 1048592 | tf_op jit(solution)/shard_map/psum | solution.py:45
  287.6 1.7 fusion.65
  289.3 1.7 fusion.48
  291.0 1.8 fusion.52
  295.9 1.7 fusion.82
  297.6 4.0 convolution_convert_fusion
  304.3 2.1 copy.27
  306.4 14.7 %all-to-all-start = ((bf16[128,32,64]{0,2,1:T(8,128)(2,1)}), bf16[128,32,64]{0,2,1:T(8,128)(2,1)S(1)}, u32[]{:S(2)}, u32[]{:S(2)}) async-start(bf16[128,32,64]{0,2,1:T(8,128)(2,1)} %bitcast.3), calls=%async_computation | async-start | bytes 1048576 | tf_op jit(solution)/shard_map/all_to_all | solution.py:142
  322.2 32.5 %all-to-all-done = bf16[128,32,64]{0,2,1:T(8,128)(2,1)S(1)} async-done(((bf16[128,32,64]{0,2,1:T(8,128)(2,1)}), bf16[128,32,64]{0,2,1:T(8,128)(2,1)S(1)}, u32[]{:S(2)}, u32[]{:S(2)}) %all-to-all-start) | async-done | bytes 524320 | tf_op jit(solution)/shard_map/all_to_all | solution.py:142
  354.6 4.2 all-to-all-start.2
  359.8 32.5 %all-to-all-done.2 = bf16[128,32,64]{0,2,1:T(8,128)(2,1)S(1)} async-done(((bf16[128,32,64]{0,2,1:T(8,128)(2,1)}), bf16[128,32,64]{0,2,1:T(8,128)(2,1)S(1)}, u32[]{:S(2)}, u32[]{:S(2)}) %all-to-all-start.2) | async-done | bytes 524320 | tf_op jit(solution)/shard_map/all_to_all | solution.py:137
  392.3 5.0 all-to-all-start.1
  398.4 22.9 %all-reduce.5.cloned.1.call-done = (bf16[128,2048]{1,0:T(8,128)(2,1)}, bf16[128,2048]{1,0:T(8,128)(2,1)}) async-done(((bf16[128,2048]{1,0:T(8,128)(2,1)}, bf16[128,2048]{1,0:T(8,128)(2,1)}), (bf16[128,2048]{1,0:T(8,128)(2,1)}, bf16[128,2048]{1,0:T(8,128)(2,1)})) %all-reduce.5.cloned.1.call-update) | async-done | bytes 1048592 | tf_op jit(solution)/shard_map/psum | solution.py:45
  422.6 8.3 %all-to-all-done.1 = bf16[128,32,64]{0,2,1:T(8,128)(2,1)} async-done(((bf16[128,32,64]{0,2,1:T(8,128)(2,1)}), bf16[128,32,64]{0,2,1:T(8,128)(2,1)}, u32[]{:S(2)}, u32[]{:S(2)}) %all-to-all-start.1) | async-done | bytes 524320 | tf_op jit(solution)/shard_map/all_to_all | solution.py:143
  430.9 6.1 %all-to-all-start.3 = ((bf16[128,32,64]{0,2,1:T(8,128)(2,1)}), bf16[128,32,64]{0,2,1:T(8,128)(2,1)S(1)}, u32[]{:S(2)}, u32[]{:S(2)}) async-start(bf16[128,32,64]{0,2,1:T(8,128)(2,1)} %bitcast.9), calls=%async_computation.3 | async-start | bytes 1048576 | tf_op jit(solution)/shard_map/all_to_all | solution.py:138
  437.1 2.7 fusion.59
  439.8 98.8 %all-gather.8.cloned.1.call-done = bf16[4096,1056]{0,1:T(8,128)(2,1)} async-done(((bf16[128,1056]{0,1:T(8,128)(2,1)}), bf16[4096,1056]{0,1:T(8,128)(2,1)}) %all-gather.8.cloned.1.call-update) | async-done | bytes 8650768 | tf_op jit(solution)/shard_map/all_gather | solution.py:11
  538.7 2.6 fusion.23
  541.2 2.6 fusion.26
  543.9 2.6 fusion.35
  546.4 2.6 fusion.38
  549.1 2.7 fusion.32
  551.8 2.6 fusion.44
  (75 shorter events, 21.7 us)
Async XLA Ops:
  7.2 80.3 %all-gather.6.cloned.1.call-start = ((), (), s32[]{:S(2)}) async-start(), calls=%async_computation.5 | async-start | bytes 1622016 | tf_op jit(solution)/shard_map/all_gather | solution.py:22
  8.7 151.3 %all-gather.4.cloned.1.call-start = ((), (), s32[]{:S(2)}) async-start(), calls=%async_computation.4 | async-start | bytes 3244032 | tf_op jit(solution)/shard_map/all_gather | solution.py:11
  10.4 277.2 %all-reduce.7.cloned.1.call-start = ((), (), s32[]{:S(2)}) async-start(), calls=%async_computation.8 | async-start | bytes 2097152 | tf_op jit(solution)/shard_map/psum | solution.py:45
  16.1 150.4 %copy-start.12 = (f32[2048]{0:T(1024)S(1)}, f32[2048]{0:T(1024)}, u32[]{:S(2)}) copy-start(f32[2048]{0:T(1024)} %param.22) | copy-start | bytes 24580
  160.0 6.5 %copy-start = (bf16[2048,704]{1,0:T(8,128)(2,1)S(1)}, bf16[2048,704]{1,0:T(8,128)(2,1)}, u32[]{:S(2)}) copy-start(bf16[2048,704]{1,0:T(8,128)(2,1)} %all-gather.4.cloned.1.call-done) | copy-start | bytes 8650756
  174.1 115.2 %copy-start.11 = (f32[2048]{0:T(1024)S(1)}, f32[2048]{0:T(1024)}, u32[]{:S(2)}) copy-start(f32[2048]{0:T(1024)} %param.23) | copy-start | bytes 24580
  174.1 247.1 %all-reduce.5.cloned.1.call-start = ((), (), s32[]{:S(2)}) async-start(), calls=%async_computation.7 | async-start | bytes 2097152 | tf_op jit(solution)/shard_map/psum | solution.py:45
  175.6 0.9 copy-start.5
  287.6 6.0 %copy-start.10 = (bf16[2048,352]{1,0:T(8,128)(2,1)S(1)}, bf16[2048,352]{1,0:T(8,128)(2,1)}, u32[]{:S(2)}) copy-start(bf16[2048,352]{1,0:T(8,128)(2,1)} %all-gather.6.cloned.1.call-done) | copy-start | bytes 4325380
  287.6 6.5 %copy-start.6 = (bf16[128,2048]{1,0:T(8,128)(2,1)S(1)}, bf16[128,2048]{1,0:T(8,128)(2,1)}, u32[]{:S(2)}) copy-start(bf16[128,2048]{1,0:T(8,128)(2,1)} %copy-done.5) | copy-start | bytes 1572868
  289.2 6.6 %copy-start.8 = (bf16[128,2048]{1,0:T(8,128)(2,1)}, bf16[128,2048]{1,0:T(8,128)(2,1)S(1)}, u32[]{:S(2)}) copy-start(bf16[128,2048]{1,0:T(8,128)(2,1)S(1)} %get-tuple-element.22) | copy-start | bytes 1572868
  292.8 0.8 copy-start.2
  303.5 17.6 %copy-start.4 = (bf16[128,2048]{1,0:T(8,128)(2,1)S(1)}, bf16[128,2048]{1,0:T(8,128)(2,1)}, u32[]{:S(2)}) copy-start(bf16[128,2048]{1,0:T(8,128)(2,1)} %fusion.47) | copy-start | bytes 1572868
  303.5 55.3 %copy-start.3 = (bf16[128,2048]{1,0:T(8,128)(2,1)S(1)}, bf16[128,2048]{1,0:T(8,128)(2,1)}, u32[]{:S(2)}) copy-start(bf16[128,2048]{1,0:T(8,128)(2,1)} %copy-done.2) | copy-start | bytes 1572868
  303.6 235.1 %all-gather.8.cloned.1.call-start = ((), (), s32[]{:S(2)}) async-start(), calls=%async_computation.6 | async-start | bytes 8921088 | tf_op jit(solution)/shard_map/all_gather | solution.py:11
  304.3 93.1 %copy-start.7 = (bf16[128,2048]{1,0:T(8,128)(2,1)S(1)}, bf16[128,2048]{1,0:T(8,128)(2,1)}, u32[]{:S(2)}) copy-start(bf16[128,2048]{1,0:T(8,128)(2,1)} %param.21) | copy-start | bytes 1572868
  306.4 114.8 %copy-start.1 = (bf16[128,2048]{1,0:T(8,128)(2,1)S(1)}, bf16[128,2048]{1,0:T(8,128)(2,1)}, u32[]{:S(2)}) copy-start(bf16[128,2048]{1,0:T(8,128)(2,1)} %param.19) | copy-start | bytes 1572868
  306.4 48.2 %all-to-all-start = ((bf16[128,32,64]{0,2,1:T(8,128)(2,1)}), bf16[128,32,64]{0,2,1:T(8,128)(2,1)S(1)}, u32[]{:S(2)}, u32[]{:S(2)}) async-start(bf16[128,32,64]{0,2,1:T(8,128)(2,1)} %bitcast.3), calls=%async_computation | async-start | bytes 1048576 | tf_op jit(solution)/shard_map/all_to_all | solution.py:142
  354.6 82.4 %copy-start.9 = (bf16[128,2048]{1,0:T(8,128)(2,1)S(1)}, bf16[128,2048]{1,0:T(8,128)(2,1)}, u32[]{:S(2)}) copy-start(bf16[128,2048]{1,0:T(8,128)(2,1)} %copy-done.8) | copy-start | bytes 1572868
  354.6 37.7 %all-to-all-start.2 = ((bf16[128,32,64]{0,2,1:T(8,128)(2,1)}), bf16[128,32,64]{0,2,1:T(8,128)(2,1)S(1)}, u32[]{:S(2)}, u32[]{:S(2)}) async-start(bf16[128,32,64]{0,2,1:T(8,128)(2,1)} %bitcast.7), calls=%async_computation.2 | async-start | bytes 1048576 | tf_op jit(solution)/shard_map/all_to_all | solution.py:137
  392.3 38.6 %all-to-all-start.1 = ((bf16[128,32,64]{0,2,1:T(8,128)(2,1)}), bf16[128,32,64]{0,2,1:T(8,128)(2,1)}, u32[]{:S(2)}, u32[]{:S(2)}) async-start(bf16[128,32,64]{0,2,1:T(8,128)(2,1)} %bitcast.5), calls=%async_computation.1 | async-start | bytes 1048576 | tf_op jit(solution)/shard_map/all_to_all | solution.py:143
  398.4 140.3 %copy-start.13 = (f32[64,176]{1,0:T(8,128)S(1)}, f32[64,176]{1,0:T(8,128)}, u32[]{:S(2)}) copy-start(f32[64,176]{1,0:T(8,128)} %param.30) | copy-start | bytes 135172
  430.9 120.8 %all-to-all-start.3 = ((bf16[128,32,64]{0,2,1:T(8,128)(2,1)}), bf16[128,32,64]{0,2,1:T(8,128)(2,1)S(1)}, u32[]{:S(2)}, u32[]{:S(2)}) async-start(bf16[128,32,64]{0,2,1:T(8,128)(2,1)} %bitcast.9), calls=%async_computation.3 | async-start | bytes 1048576 | tf_op jit(solution)/shard_map/all_to_all | solution.py:138
  437.0 104.2 %copy-start.14 = (f32[64,176]{1,0:T(8,128)S(1)}, f32[64,176]{1,0:T(8,128)}, u32[]{:S(2)}) copy-start(f32[64,176]{1,0:T(8,128)} %param.31) | copy-start | bytes 135172
  439.8 104.0 %copy-start.15 = (f32[64,176]{1,0:T(8,128)S(1)}, f32[64,176]{1,0:T(8,128)}, u32[]{:S(2)}) copy-start(f32[64,176]{1,0:T(8,128)} %param.33) | copy-start | bytes 135172
  439.8 106.6 %copy-start.16 = (f32[64,176]{1,0:T(8,128)S(1)}, f32[64,176]{1,0:T(8,128)}, u32[]{:S(2)}) copy-start(f32[64,176]{1,0:T(8,128)} %param.34) | copy-start | bytes 135172
  541.2 7.8 %copy-start.17 = (f32[176,64]{0,1:T(8,128)S(1)}, f32[176,64]{0,1:T(8,128)}, u32[]{:S(2)}) copy-start(f32[176,64]{0,1:T(8,128)} %param.32) | copy-start | bytes 135172
  546.4 5.3 copy-start.18
Sparse Core Ops, SparseCore 0:
  10.7 76.7 all-gather.5
  90.1 69.8 all-gather.3
  174.2 113.2 all-reduce.6
  303.7 117.5 all-reduce.4
  423.1 115.4 all-gather.7
where the time goes:
time: 562 us; the launch traced here: 561 us
  waiting for transfers between devices  447 us (80%)
  matrix products  41.5 us (7%)
  starting transfers between devices  30.4 us (5%)
  other arithmetic  22 us (4%)
  between operations  14 us (2%)
  local copies, waits for them, and re-layouts  6.1 us (1%)
    all_gather x2, waiting for transfers between devices, sent_together(): whole, at, outs = (lax.all_gather(both, axis, axis=dim, tiled=True), 0, [])  169 us
    psum x2, waiting for transfers between devices, block_forward(): lax.psum(jnp.dot(hidden, w_down, preferred_element_type=jnp.float32).asty...  133 us
    all_gather x1, waiting for transfers between devices, gather_turned(): whole = lax.all_gather(both, axis, axis=0, tiled=True)  71.3 us
    all_to_all x1, waiting for transfers between devices, per_device(): lax.all_to_all(saved_second[0], 'fs', split_axis=1, concat_axis=0, tiled=...  32.5 us
    all_to_all x1, waiting for transfers between devices, per_device(): lax.all_to_all(saved_first[0], 'fs', split_axis=1, concat_axis=0, tiled=T...  32.5 us
    all_to_all x1, starting transfers between devices, per_device(): lax.all_to_all(saved_first[0], 'fs', split_axis=1, concat_axis=0, tiled=T...  14.7 us
  transfers between devices with their start and end apart: 9, of which 8 were waited for; matrix products, arithmetic and copies ran while one was open for 6% of the time, Pallas kernels for 0%

commit v1 on v0

--- a/solution.py
+++ b/solution.py
@@ -134,7 +134,12 @@
     )
     upper = fold_block(
         pieces[0:3],
-        lax.all_to_all(saved_second[0], "fs", split_axis=1, concat_axis=0, tiled=True),
+        jnp.concatenate(
+            lax.all_to_all(
+                jnp.stack(jnp.split(saved_second[0], lax.axis_size("fs"), axis=1)), "fs", 0, 0
+            ),
+            axis=0,
+        ),
         lax.all_to_all(saved_second[1], "fs", split_axis=1, concat_axis=0, tiled=True),
     )
     lower = fold_block(

time: 562 us -> 562 us (level)
  transfers between devices with their start and end apart: 9 -> 9, of which waited for: 8 -> 8; matrix products, arithmetic and copies ran while one was open for 6% -> 7% of each run, Pallas kernels for 0% -> 0%
where the time goes in v1:
time: 562 us; the launch traced here: 561 us
  waiting for transfers between devices  445 us (79%)
  matrix products  41.7 us (7%)
  starting transfers between devices  30.4 us (5%)
  other arithmetic  22 us (4%)
  between operations  14.2 us (3%)
  local copies, waits for them, and re-layouts  7.94 us (1%)
    all_gather x2, waiting for transfers between devices, sent_together(): whole, at, outs = (lax.all_gather(both, axis, axis=dim, tiled=True), 0, [])  169 us
    psum x2, waiting for transfers between devices, block_forward(): lax.psum(jnp.dot(hidden, w_down, preferred_element_type=jnp.float32).asty...  134 us
    all_gather x1, waiting for transfers between devices, gather_turned(): whole = lax.all_gather(both, axis, axis=0, tiled=True)  71.3 us
    all_to_all x1, waiting for transfers between devices, per_device(): lax.all_to_all(jnp.stack(jnp.split(saved_second[0], lax.axis_size('fs'),...  32.5 us
    all_to_all x1, waiting for transfers between devices, per_device(): lax.all_to_all(saved_first[0], 'fs', split_axis=1, concat_axis=0, tiled=T...  30.5 us
    all_to_all x1, starting transfers between devices, per_device(): lax.all_to_all(saved_first[0], 'fs', split_axis=1, concat_axis=0, tiled=T...  14.7 us
  transfers between devices with their start and end apart: 9, of which 8 were waited for; matrix products, arithmetic and copies ran while one was open for 7% of the time, Pallas kernels for 0%

profile of v1, /device:TPU:1, one launch (start us, length us, event | category | flops | bytes accessed | tf_op | source)
XLA Modules:
  0.0 561.1 jit_solution(13184744212215624590)
XLA Ops:
  8.8 1.6 pad_maximum_fusion
  14.1 2.0 fusion.47
  16.1 71.3 %all-gather.6.cloned.1.call-done = bf16[2048,352]{1,0:T(8,128)(2,1)} async-done(((bf16[64,352]{1,0:T(8,128)(2,1)}), bf16[2048,352]{1,0:T(8,128)(2,1)}) %all-gather.6.cloned.1.call-update) | async-done | bytes 1441808 | tf_op jit(solution)/shard_map/all_gather | solution.py:22
  87.5 2.1 fusion.20
  89.6 70.4 %all-gather.4.cloned.1.call-done = bf16[2048,704]{1,0:T(8,128)(2,1)} async-done(((bf16[64,704]{1,0:T(8,128)(2,1)}), bf16[2048,704]{1,0:T(8,128)(2,1)}) %all-gather.4.cloned.1.call-update) | async-done | bytes 2883600 | tf_op jit(solution)/shard_map/all_gather | solution.py:11
  160.0 2.6 fusion.74
  162.6 3.2 constant_dynamic-update-slice_fusion.5
  166.5 1.6 fusion.93
  168.1 3.9 convolution_convert_fusion.1
  177.5 110.1 %all-reduce.7.cloned.1.call-done = (bf16[128,2048]{1,0:T(8,128)(2,1)}, bf16[128,2048]{1,0:T(8,128)(2,1)}) async-done(((bf16[128,2048]{1,0:T(8,128)(2,1)}, bf16[128,2048]{1,0:T(8,128)(2,1)}), (bf16[128,2048]{1,0:T(8,128)(2,1)}, bf16[128,2048]{1,0:T(8,128)(2,1)})) %all-reduce.7.cloned.1.call-update) | async-done | bytes 1048592 | tf_op jit(solution)/shard_map/psum | solution.py:45
  287.6 1.7 fusion.65
  289.3 1.7 fusion.48
  291.0 1.8 fusion.52
  295.9 1.7 fusion.82
  297.6 4.0 convolution_convert_fusion
  304.3 2.0 copy.40
  306.4 14.7 %all-to-all-start = ((bf16[128,32,64]{0,2,1:T(8,128)(2,1)}), bf16[128,32,64]{0,2,1:T(8,128)(2,1)}, u32[]{:S(2)}, u32[]{:S(2)}) async-start(bf16[128,32,64]{0,2,1:T(8,128)(2,1)} %bitcast.3), calls=%async_computation | async-start | bytes 1048576 | tf_op jit(solution)/shard_map/all_to_all | solution.py:147
  324.2 30.5 %all-to-all-done = bf16[128,32,64]{0,2,1:T(8,128)(2,1)} async-done(((bf16[128,32,64]{0,2,1:T(8,128)(2,1)}), bf16[128,32,64]{0,2,1:T(8,128)(2,1)}, u32[]{:S(2)}, u32[]{:S(2)}) %all-to-all-start) | async-done | bytes 524320 | tf_op jit(solution)/shard_map/all_to_all | solution.py:147
  354.7 4.0 all-to-all-start.2
  359.8 32.5 %all-to-all-done.2 = bf16[32,128,64]{1,2,0:T(8,128)(2,1)S(1)} async-done(((bf16[32,128,64]{1,2,0:T(8,128)(2,1)}), bf16[32,128,64]{1,2,0:T(8,128)(2,1)S(1)}, u32[]{:S(2)}, u32[]{:S(2)}) %all-to-all-start.2) | async-done | bytes 524320 | tf_op jit(solution)/shard_map/all_to_all | solution.py:138
  392.3 4.3 all-to-all-start.1
  397.7 23.6 %all-reduce.5.cloned.1.call-done = (bf16[128,2048]{1,0:T(8,128)(2,1)}, bf16[128,2048]{1,0:T(8,128)(2,1)}) async-done(((bf16[128,2048]{1,0:T(8,128)(2,1)}, bf16[128,2048]{1,0:T(8,128)(2,1)}), (bf16[128,2048]{1,0:T(8,128)(2,1)}, bf16[128,2048]{1,0:T(8,128)(2,1)})) %all-reduce.5.cloned.1.call-update) | async-done | bytes 1048592 | tf_op jit(solution)/shard_map/psum | solution.py:45
  422.6 7.5 %all-to-all-done.1 = bf16[128,32,64]{0,2,1:T(8,128)(2,1)S(1)} async-done(((bf16[128,32,64]{0,2,1:T(8,128)(2,1)}), bf16[128,32,64]{0,2,1:T(8,128)(2,1)S(1)}, u32[]{:S(2)}, u32[]{:S(2)}) %all-to-all-start.1) | async-done | bytes 524320 | tf_op jit(solution)/shard_map/all_to_all | solution.py:148
  430.2 6.9 %all-to-all-start.3 = ((bf16[128,32,64]{0,2,1:T(8,128)(2,1)}), bf16[128,32,64]{0,2,1:T(8,128)(2,1)S(1)}, u32[]{:S(2)}, u32[]{:S(2)}) async-start(bf16[128,32,64]{0,2,1:T(8,128)(2,1)} %bitcast.39), calls=%async_computation.3 | async-start | bytes 1048576 | tf_op jit(solution)/shard_map/all_to_all | solution.py:143
  437.1 2.7 fusion.59
  439.8 98.8 %all-gather.8.cloned.1.call-done = bf16[4096,1056]{0,1:T(8,128)(2,1)} async-done(((bf16[128,1056]{0,1:T(8,128)(2,1)}), bf16[4096,1056]{0,1:T(8,128)(2,1)}) %all-gather.8.cloned.1.call-update) | async-done | bytes 8650768 | tf_op jit(solution)/shard_map/all_gather | solution.py:11
  538.7 2.8 fusion.23
  541.4 2.8 fusion.26
  544.2 2.6 fusion.35
  546.8 2.6 fusion.38
  549.4 2.6 fusion.32
  552.0 2.6 fusion.44
  (107 shorter events, 23.6 us)
Async XLA Ops:
  7.2 80.3 %all-gather.6.cloned.1.call-start = ((), (), s32[]{:S(2)}) async-start(), calls=%async_computation.5 | async-start | bytes 1622016 | tf_op jit(solution)/shard_map/all_gather | solution.py:22
  8.7 151.3 %all-gather.4.cloned.1.call-start = ((), (), s32[]{:S(2)}) async-start(), calls=%async_computation.4 | async-start | bytes 3244032 | tf_op jit(solution)/shard_map/all_gather | solution.py:11
  10.4 277.3 %all-reduce.7.cloned.1.call-start = ((), (), s32[]{:S(2)}) async-start(), calls=%async_computation.8 | async-start | bytes 2097152 | tf_op jit(solution)/shard_map/psum | solution.py:45
  16.1 150.4 %copy-start.12 = (f32[2048]{0:T(1024)S(1)}, f32[2048]{0:T(1024)}, u32[]{:S(2)}) copy-start(f32[2048]{0:T(1024)} %param.22) | copy-start | bytes 24580
  160.0 6.5 %copy-start = (bf16[2048,704]{1,0:T(8,128)(2,1)S(1)}, bf16[2048,704]{1,0:T(8,128)(2,1)}, u32[]{:S(2)}) copy-start(bf16[2048,704]{1,0:T(8,128)(2,1)} %all-gather.4.cloned.1.call-done) | copy-start | bytes 8650756
  174.1 115.2 %copy-start.11 = (f32[2048]{0:T(1024)S(1)}, f32[2048]{0:T(1024)}, u32[]{:S(2)}) copy-start(f32[2048]{0:T(1024)} %param.23) | copy-start | bytes 24580
  174.1 247.1 %all-reduce.5.cloned.1.call-start = ((), (), s32[]{:S(2)}) async-start(), calls=%async_computation.7 | async-start | bytes 2097152 | tf_op jit(solution)/shard_map/psum | solution.py:45
  175.6 0.9 copy-start.5
  287.6 6.0 %copy-start.10 = (bf16[2048,352]{1,0:T(8,128)(2,1)S(1)}, bf16[2048,352]{1,0:T(8,128)(2,1)}, u32[]{:S(2)}) copy-start(bf16[2048,352]{1,0:T(8,128)(2,1)} %all-gather.6.cloned.1.call-done) | copy-start | bytes 4325380
  287.6 6.5 %copy-start.6 = (bf16[128,2048]{1,0:T(8,128)(2,1)S(1)}, bf16[128,2048]{1,0:T(8,128)(2,1)}, u32[]{:S(2)}) copy-start(bf16[128,2048]{1,0:T(8,128)(2,1)} %copy-done.5) | copy-start | bytes 1572868
  289.3 6.6 %copy-start.8 = (bf16[128,2048]{1,0:T(8,128)(2,1)}, bf16[128,2048]{1,0:T(8,128)(2,1)S(1)}, u32[]{:S(2)}) copy-start(bf16[128,2048]{1,0:T(8,128)(2,1)S(1)} %get-tuple-element.22) | copy-start | bytes 1572868
  292.8 0.8 copy-start.3
  303.6 17.5 %copy-start.1 = (bf16[128,2048]{1,0:T(8,128)(2,1)S(1)}, bf16[128,2048]{1,0:T(8,128)(2,1)}, u32[]{:S(2)}) copy-start(bf16[128,2048]{1,0:T(8,128)(2,1)} %fusion.47) | copy-start | bytes 1572868
  303.6 235.0 %all-gather.8.cloned.1.call-start = ((), (), s32[]{:S(2)}) async-start(), calls=%async_computation.6 | async-start | bytes 8921088 | tf_op jit(solution)/shard_map/all_gather | solution.py:11
  306.4 52.4 %copy-start.4 = (bf16[128,2048]{1,0:T(8,128)(2,1)S(1)}, bf16[128,2048]{1,0:T(8,128)(2,1)}, u32[]{:S(2)}) copy-start(bf16[128,2048]{1,0:T(8,128)(2,1)} %copy-done.3) | copy-start | bytes 1572868
  306.4 48.3 %all-to-all-start = ((bf16[128,32,64]{0,2,1:T(8,128)(2,1)}), bf16[128,32,64]{0,2,1:T(8,128)(2,1)}, u32[]{:S(2)}, u32[]{:S(2)}) async-start(bf16[128,32,64]{0,2,1:T(8,128)(2,1)} %bitcast.3), calls=%async_computation | async-start | bytes 1048576 | tf_op jit(solution)/shard_map/all_to_all | solution.py:147
  321.6 75.0 %copy-start.7 = (bf16[128,2048]{1,0:T(8,128)(2,1)S(1)}, bf16[128,2048]{1,0:T(8,128)(2,1)}, u32[]{:S(2)}) copy-start(bf16[128,2048]{1,0:T(8,128)(2,1)} %param.21) | copy-start | bytes 1572868
  322.6 98.6 %copy-start.2 = (bf16[128,2048]{1,0:T(8,128)(2,1)S(1)}, bf16[128,2048]{1,0:T(8,128)(2,1)}, u32[]{:S(2)}) copy-start(bf16[128,2048]{1,0:T(8,128)(2,1)} %param.19) | copy-start | bytes 1572868
  324.2 112.8 %copy-start.9 = (bf16[128,2048]{1,0:T(8,128)(2,1)S(1)}, bf16[128,2048]{1,0:T(8,128)(2,1)}, u32[]{:S(2)}) copy-start(bf16[128,2048]{1,0:T(8,128)(2,1)} %copy-done.8) | copy-start | bytes 1572868
  354.7 37.6 %all-to-all-start.2 = ((bf16[32,128,64]{1,2,0:T(8,128)(2,1)}), bf16[32,128,64]{1,2,0:T(8,128)(2,1)S(1)}, u32[]{:S(2)}, u32[]{:S(2)}) async-start(bf16[32,128,64]{1,2,0:T(8,128)(2,1)} %copy.44), calls=%async_computation.2 | async-start | bytes 1048576 | tf_op jit(solution)/shard_map/all_to_all | solution.py:138
  392.3 37.9 %all-to-all-start.1 = ((bf16[128,32,64]{0,2,1:T(8,128)(2,1)}), bf16[128,32,64]{0,2,1:T(8,128)(2,1)S(1)}, u32[]{:S(2)}, u32[]{:S(2)}) async-start(bf16[128,32,64]{0,2,1:T(8,128)(2,1)} %bitcast.5), calls=%async_computation.1 | async-start | bytes 1048576 | tf_op jit(solution)/shard_map/all_to_all | solution.py:148
  397.6 141.0 %copy-start.13 = (f32[64,176]{1,0:T(8,128)S(1)}, f32[64,176]{1,0:T(8,128)}, u32[]{:S(2)}) copy-start(f32[64,176]{1,0:T(8,128)} %param.30) | copy-start | bytes 135172
  430.2 121.8 %all-to-all-start.3 = ((bf16[128,32,64]{0,2,1:T(8,128)(2,1)}), bf16[128,32,64]{0,2,1:T(8,128)(2,1)S(1)}, u32[]{:S(2)}, u32[]{:S(2)}) async-start(bf16[128,32,64]{0,2,1:T(8,128)(2,1)} %bitcast.39), calls=%async_computation.3 | async-start | bytes 1048576 | tf_op jit(solution)/shard_map/all_to_all | solution.py:143
  437.0 104.4 %copy-start.14 = (f32[64,176]{1,0:T(8,128)S(1)}, f32[64,176]{1,0:T(8,128)}, u32[]{:S(2)}) copy-start(f32[64,176]{1,0:T(8,128)} %param.31) | copy-start | bytes 135172
  439.8 104.4 %copy-start.15 = (f32[64,176]{1,0:T(8,128)S(1)}, f32[64,176]{1,0:T(8,128)}, u32[]{:S(2)}) copy-start(f32[64,176]{1,0:T(8,128)} %param.33) | copy-start | bytes 135172
  439.8 107.0 %copy-start.16 = (f32[64,176]{1,0:T(8,128)S(1)}, f32[64,176]{1,0:T(8,128)}, u32[]{:S(2)}) copy-start(f32[64,176]{1,0:T(8,128)} %param.34) | copy-start | bytes 135172
  541.4 8.0 %copy-start.17 = (f32[176,64]{0,1:T(8,128)S(1)}, f32[176,64]{0,1:T(8,128)}, u32[]{:S(2)}) copy-start(f32[176,64]{0,1:T(8,128)} %param.32) | copy-start | bytes 135172
  546.8 5.2 copy-start.18
Sparse Core Ops, SparseCore 0:
  10.7 76.7 all-gather.5
  90.1 69.8 all-gather.3
  174.3 113.3 all-reduce.6
  303.7 117.4 all-reduce.4
  423.1 115.4 all-gather.7
